TPU v7x, 32 devices: a whole 2x2x4 slice. The times are simulated.
32 devices in a mesh: ep: 16 (over z, y, x), tp: 2 (over core).
Axes of the slice: x: 2, y: 2, z: 4, core: 2. Of those that a mesh axis runs over, the one named last changes fastest.
Arguments:
- tokens: bfloat16 [256, 2048], P('ep'), may hold values from -6 to 6
- mix_gain: float32 [2048], replicated, may hold values from 0.1 to 1.9
- w_query: bfloat16 [2048, 1024], P(None, 'tp'), may hold values from -0.125 to 0.125
- w_forget: bfloat16 [2048, 1024], P(None, 'tp'), may hold values from -0.125 to 0.125
- w_input: bfloat16 [2048, 1024], P(None, 'tp'), may hold values from -0.125 to 0.125
- w_outgate: bfloat16 [2048, 1024], P(None, 'tp'), may hold values from -0.125 to 0.125
- decay_floor: float32 [1024], P('tp'), may hold values from 0 to 0.9
- head_gain: float32 [128], replicated, may hold values from 0.1 to 1.9
- prev_state: float32 [256, 8, 128, 128], P('ep', 'tp'), may hold values from -4 to 4
- w_output: bfloat16 [1024, 2048], P('tp'), may hold values from -0.1875 to 0.1875
- moe_gain: float32 [2048], replicated, may hold values from 0.1 to 1.9
- route_ids: int32 [256, 2], P('ep'), may hold values from 0 to 7, all different within a row; in each aligned block of 16 rows (0 to 15, 16 to 31, ...) at most 16 rows name the same one
- route_logits: float32 [256, 2], P('ep'), may hold values from -6 to 6
- w_exp_gate: bfloat16 [16, 2048, 1536], P('ep', None, 'tp'), may hold values from -0.125 to 0.125
- w_exp_up: bfloat16 [16, 2048, 1536], P('ep', None, 'tp'), may hold values from -0.125 to 0.125
- w_exp_down: bfloat16 [16, 1536, 2048], P('ep', 'tp'), may hold values from -0.109375 to 0.109375
Outputs:
- layer_out: bfloat16 [256, 2048], P('ep')
- new_state: float32 [256, 8, 128, 128], P('ep', 'tp')
Inputs may be any that keep to these rules, and one draw needn't show every extreme that they name: `route_ids`: each row names 2 different experts; within the rows of one device no expert is named more than 16 times, and in every draw some expert is named exactly 16 times in some device's rows.
All inputs are finite; a program needn't handle non-finite values.
Results may differ from a plain program's by a relative error of at most 0.014.
Values may be sent and summed in bfloat16 or wider, within the bound.
A program may use at most 128 MiB of HBM per device.

v0:
```python
import jax
import jax.numpy as jnp
from jax import lax
from jax.sharding import PartitionSpec as P

TOP_K = 2
epsilon = 1e-06


def rms_scale(values, gains):
    return values * lax.rsqrt(jnp.mean(values * values, axis=-1, keepdims=True) + epsilon) * gains


def on_device(
    tokens,
    mix_gain,
    w_query,
    w_forget,
    w_input,
    w_outgate,
    decay_floor,
    head_gain,
    prev_state,
    w_output,
    moe_gain,
    route_ids,
    route_logits,
    w_exp_gate,
    w_exp_up,
    w_exp_down,
):
    seq_dev = tokens.shape[0]
    ep_size = lax.axis_size("ep")
    residual = tokens.astype(jnp.float32)
    normed = rms_scale(residual, mix_gain).astype(jnp.bfloat16)
    heads_dev = prev_state.shape[1]
    head_dim = prev_state.shape[2]
    head_width = heads_dev * head_dim
    query_part = jnp.dot(normed, w_query, preferred_element_type=jnp.float32).reshape(
        seq_dev, heads_dev, head_dim
    )
    forget_pre = jnp.dot(normed, w_forget, preferred_element_type=jnp.float32).reshape(
        seq_dev, heads_dev, head_dim
    )
    value_part = jnp.dot(normed, w_input, preferred_element_type=jnp.float32).reshape(
        seq_dev, heads_dev, head_dim
    )
    outgate_pre = jnp.dot(normed, w_outgate, preferred_element_type=jnp.float32).reshape(
        seq_dev, heads_dev, head_dim
    )
    floor_rate = decay_floor.reshape(heads_dev, head_dim)
    forget = floor_rate + (1.0 - floor_rate) * jax.nn.sigmoid(forget_pre)
    key_part = (1.0 - floor_rate) * jax.nn.sigmoid(-forget_pre)
    new_state = forget[..., None] * prev_state + key_part[..., None] * value_part[:, :, None, :]
    readout = jnp.sum(query_part[..., None] * new_state, axis=2)
    gated = (
        (rms_scale(readout, head_gain) * jax.nn.silu(outgate_pre))
        .reshape(seq_dev, head_width)
        .astype(jnp.bfloat16)
    )
    mixed_out = lax.psum(
        jnp.dot(gated, w_output, preferred_element_type=jnp.float32).astype(jnp.bfloat16), "tp"
    ).astype(jnp.float32)
    middle = (residual + mixed_out).astype(jnp.bfloat16)
    normed_two = rms_scale(middle.astype(jnp.float32), moe_gain).astype(jnp.bfloat16)
    experts = ep_size // 2
    capacity = min(seq_dev, max(2, 8 * seq_dev * TOP_K // experts))
    slot_total = ep_size * capacity
    pair_expert = route_ids.reshape(-1)
    onehot = (pair_expert[:, None] == jnp.arange(experts, dtype=jnp.int32)[None, :]).astype(
        jnp.int32
    )
    slot_rank = jnp.sum((jnp.cumsum(onehot, axis=0) - onehot) * onehot, axis=1)
    slot_ids = jnp.arange(slot_total, dtype=jnp.int32)
    slot_expert = slot_ids // capacity // 2
    slot_order = slot_ids % capacity
    matches = (slot_expert[:, None] == pair_expert[None, :]) & (
        slot_order[:, None] == slot_rank[None, :]
    )
    match_tok = jnp.any(matches.reshape(slot_total, seq_dev, TOP_K), axis=2)
    outgoing = (
        jnp.dot(match_tok.astype(jnp.bfloat16), normed_two, preferred_element_type=jnp.float32)
        .astype(jnp.bfloat16)
        .reshape(ep_size, capacity, -1)
    )
    arrived = lax.all_to_all(outgoing, "ep", split_axis=0, concat_axis=0, tiled=True)
    per_source = arrived.shape[1]
    slot_rows = arrived.reshape(ep_size * per_source, arrived.shape[2])
    gate_pre = jnp.dot(slot_rows, w_exp_gate[0], preferred_element_type=jnp.float32)
    up_pre = jnp.dot(slot_rows, w_exp_up[0], preferred_element_type=jnp.float32)
    activated = (jax.nn.silu(gate_pre) * up_pre).astype(jnp.bfloat16)
    partial_down = jnp.dot(activated, w_exp_down[0], preferred_element_type=jnp.float32)
    share = lax.psum_scatter(
        partial_down.astype(jnp.bfloat16), "tp", scatter_dimension=1, tiled=True
    )
    answer = share.reshape(ep_size, per_source, -1)
    returned = lax.all_to_all(answer, "ep", split_axis=0, concat_axis=0, tiled=True)
    returned = lax.all_gather(returned, "tp", axis=2, tiled=True)
    weights = jax.nn.sigmoid(route_logits - jnp.flip(route_logits, axis=1)).reshape(-1)
    combine = jnp.sum(
        (matches.astype(jnp.float32) * weights[None, :]).reshape(slot_total, seq_dev, TOP_K), axis=2
    ).T
    expert_sum = jnp.dot(
        combine,
        returned.reshape(slot_total, -1).astype(jnp.float32),
        precision=lax.Precision.HIGHEST,
    )
    layer_out = (middle.astype(jnp.float32) + expert_sum).astype(jnp.bfloat16)
    return (layer_out, new_state)


def solution(mesh):
    placed = (
        P("ep", None),
        P(),
        P(None, "tp"),
        P(None, "tp"),
        P(None, "tp"),
        P(None, "tp"),
        P("tp"),
        P(),
        P("ep", "tp", None, None),
        P("tp", None),
        P(),
        P("ep", None),
        P("ep", None),
        P("ep", None, "tp"),
        P("ep", None, "tp"),
        P("ep", "tp", None),
    )
    return jax.shard_map(
        on_device,
        mesh=mesh,
        in_specs=placed,
        out_specs=(P("ep", None), P("ep", "tp", None, None)),
        check_vma=False,
    )
```

profile of v0, /device:TPU:0, one launch (start us, length us, event | category | flops | bytes accessed | tf_op | source)
XLA Modules:
  0.0 138.2 jit_solution(3309153512424318484)
XLA Ops:
  7.2 0.0 copy-start
  7.2 0.0 copy-start.1
  7.2 0.0 copy-start.4
  7.2 0.0 all-reduce.2.cloned.1.call-start
  7.2 1.1 fusion.19
  8.4 0.0 copy-start.7
  8.4 2.1 %add_divide_fusion.1 = (f32[16,512]{1,0:T(8,128)S(1)}, f32[16,512]{1,0:T(8,128)S(1)}) fusion(bf16[2048,512]{1,0:T(8,128)(2,1)} %param.19, bf16[16,2048]{1,0:T(8,128)(2,1)} %param.16, f32[2048]{0:T(1024)} %param.17, f32[16]{0:T(128)S(1)} %add_rsqrt_fusion.2), kind=kOutput, calls=%fused_computation.37 | convolution fusion | flops 33726464 | bytes 2236480 | tf_op jit(solution)/shard_map/dot_general | solution.py:42
  10.5 0.7 broadcast_subtract_fusion
  11.2 2.1 %fusion.47 = f32[16,512]{1,0:T(8,128)S(1)} fusion(bf16[2048,512]{1,0:T(8,128)(2,1)} %param.18, bf16[16,2048]{1,0:T(8,128)(2,1)} %param.16, f32[2048]{0:T(1024)} %param.17, f32[16]{0:T(128)S(1)} %add_rsqrt_fusion.2), kind=kOutput, calls=%fused_computation.69 | convolution fusion | flops 33685504 | bytes 2203712 | tf_op jit(solution)/shard_map/dot_general | solution.py:39
  13.3 0.0 copy-done.1
  13.3 0.0 copy-done.4
  13.3 2.0 %fusion.43 = f32[16,512]{1,0:T(8,128)S(1)} fusion(bf16[2048,512]{1,0:T(8,128)(2,1)} %param.20, bf16[16,2048]{1,0:T(8,128)(2,1)S(1)} %copy-done.1, f32[2048]{0:T(1024)S(1)} %copy-done.4, f32[16]{0:T(128)S(1)} %add_rsqrt_fusion.2), kind=kOutput, calls=%fused_computation.67 | convolution fusion | flops 33685504 | bytes 2203712 | tf_op jit(solution)/shard_map/dot_general | solution.py:45
  15.4 0.0 copy-done.7
  15.4 0.0 copy-start.9
  15.4 8.1 %multiply_reduce_fusion = (f32[16,4,128]{2,1,0:T(4,128)S(1)}, f32[16,4,128,128]{3,2,1,0:T(8,128)}) fusion(f32[16,4,128]{2,1,0:T(4,128)S(1)} %mul.153, f32[16,4,128]{2,1,0:T(4,128)S(1)} %mul.161, f32[16,4,128]{2,1,0:T(4,128)S(1)} %bitcast.55, f32[16,4,128,128]{3,2,1,0:T(8,128)} %param.24, f32[16,4,128]{2,1,0:T(4,128)S(1)} %bitcast.54), kind=kLoop, calls=%fused_computation | loop fusion | flops 5234688 | bytes 8552448 | tf_op jit(solution)/shard_map/reduce_sum | solution.py:55
  23.5 0.0 copy-start.5
  23.6 0.0 copy-start.6
  23.6 0.1 multiply_reduce_fusion.1
  23.7 0.1 broadcast_multiply_fusion
  23.8 0.0 copy-done.9
  23.8 3.7 %convolution_convert_fusion.1 = bf16[16,2048]{1,0:T(8,128)(2,1)} fusion(bf16[512,2048]{1,0:T(8,128)(2,1)} %param.25, f32[2,8,4,128]{3,2,1,0:T(4,128)S(1)} %bitcast.56, f32[512]{0:T(512)S(1)} %broadcast_bitcast_fusion, bf16[2048,512]{1,0:T(8,128)(2,1)} %param.21, bf16[16,2048]{1,0:T(8,128)(2,1)S(1)} %copy-done.1, f32[2048]{0:T(1024)S(1)} %copy-done.4, ...), kind=kOutput, calls=%fused_computation.12 | convolution fusion | flops 67330048 | bytes 4368448 | tf_op jit(solution)/shard_map/dot_general | solution.py:62
  27.4 0.0 all-reduce.2.cloned.1.call-update
  27.5 0.0 reduce-scatter.2.cloned.1.call-start
  27.5 0.0 copy-done.5
  27.5 0.1 copy.24
  27.6 0.1 eq.53
  27.7 0.1 fusion.33
  27.8 0.1 reduce_window_sum.11
  27.8 0.2 select_reduce_fusion.1
  28.0 0.1 eq.57
  28.1 0.1 copy.25
  28.2 0.1 fusion.31
  28.3 19.8 %all-reduce.2.cloned.1.call-done = bf16[16,2048]{1,0:T(8,128)(2,1)} async-done(((bf16[16,2048]{1,0:T(8,128)(2,1)}), bf16[16,2048]{1,0:T(8,128)(2,1)}) %all-reduce.2.cloned.1.call-update) | async-done | bytes 65552 | tf_op jit(solution)/shard_map/psum | solution.py:61
  48.1 0.0 copy-start.10
  48.1 1.1 fusion.23
  49.2 0.0 copy-done.6
  49.2 1.3 convolution_convert_fusion
  50.5 33.3 %all_to_all.10 = bf16[16,16,2048]{2,1,0:T(8,128)(2,1)S(1)} all-to-all(bf16[16,16,2048]{2,1,0:T(8,128)(2,1)S(1)} %bitcast.49), channel_id=1, replica_groups=mesh['ep'=16,'tp'=2] {'ep'}, dimensions={0} | all-to-all | bytes 2097152 | tf_op jit(solution)/shard_map/all_to_all | solution.py:86
  83.9 0.0 copy-start.2
  83.9 1.0 copy-done.2
  84.9 0.0 copy-done.10
  84.9 1.9 %fusion.4 = f32[256,768]{1,0:T(8,128)} fusion(bf16[256,2048]{1,0:T(8,128)(2,1)S(1)} %bitcast.51, bf16[1,2048,768]{2,1,0:T(8,128)(2,1)S(1)} %copy-done.10), kind=kOutput, calls=%fused_computation.6 | convolution fusion | flops 805306368 | bytes 4980736 | tf_op jit(solution)/shard_map/dot_general | solution.py:89
  86.8 0.0 copy-done
  86.8 0.0 copy-start.8
  86.8 0.0 copy-start.3
  86.8 5.5 %fusion.6 = bf16[256,2048]{1,0:T(8,128)(2,1)} fusion(bf16[1,768,2048]{2,1,0:T(8,128)(2,1)S(1)} %copy-done, bf16[256,2048]{1,0:T(8,128)(2,1)} %bitcast.52, bf16[1,2048,768]{2,1,0:T(8,128)(2,1)} %param.30, f32[256,768]{1,0:T(8,128)} %fusion.4), kind=kOutput, calls=%fused_computation.9 | convolution fusion | flops 1612316672 | bytes 9175040 | tf_op jit(solution)/shard_map/dot_general | solution.py:92
  92.3 0.0 reduce-scatter.2.cloned.1.call-update
  92.4 0.0 all-gather.2.cloned.1.call-start
  92.4 6.8 %reduce-scatter.2.cloned.1.call-done = bf16[256,1024]{1,0:T(8,128)(2,1)} async-done(((bf16[256,2048]{1,0:T(8,128)(2,1)}), bf16[256,1024]{1,0:T(8,128)(2,1)}) %reduce-scatter.2.cloned.1.call-update) | async-done | bytes 524304 | tf_op jit(solution)/shard_map/reduce_scatter | solution.py:93
  99.3 22.4 %all_to_all.11 = bf16[16,16,1024]{2,1,0:T(8,128)(2,1)} all-to-all(bf16[16,16,1024]{2,1,0:T(8,128)(2,1)} %bitcast.53), channel_id=1, replica_groups=mesh['ep'=16,'tp'=2] {'ep'}, dimensions={0} | all-to-all | bytes 1048576 | tf_op jit(solution)/shard_map/all_to_all | solution.py:97
  121.6 0.0 all-gather.2.cloned.1.call-update
  121.7 0.0 copy-done.8
  121.7 0.1 select_reduce_fusion
  121.8 7.4 %all-gather.2.cloned.1.call-done = bf16[16,16,2048]{2,1,0:T(8,128)(2,1)} async-done(((bf16[16,16,1024]{2,1,0:T(8,128)(2,1)}), bf16[16,16,2048]{2,1,0:T(8,128)(2,1)}) %all-gather.2.cloned.1.call-update) | async-done | bytes 1048592 | tf_op jit(solution)/shard_map/all_gather | solution.py:98
  129.2 0.0 copy-done.3
  129.2 2.4 %fusion.9 = bf16[16,2048]{1,0:T(8,128)(2,1)} fusion(f32[256,16]{0,1:T(8,128)S(1)} %select_reduce_fusion, bf16[256,2048]{1,0:T(8,128)(2,1)} %bitcast.50, bf16[16,2048]{1,0:T(8,128)(2,1)S(1)} %copy-done.3, bf16[16,2048]{1,0:T(8,128)(2,1)S(1)} %copy-done.1), kind=kOutput, calls=%fused_computation.11 | convolution fusion | flops 100892672 | bytes 1261568 | tf_op jit(solution)/shard_map/dot_general | solution.py:103
  (14 shorter events, 0.1 us)
Async XLA Ops:
  7.2 79.6 %copy-start = (bf16[1,768,2048]{2,1,0:T(8,128)(2,1)S(1)}, bf16[1,768,2048]{2,1,0:T(8,128)(2,1)}, u32[]{:S(2)}) copy-start(bf16[1,768,2048]{2,1,0:T(8,128)(2,1)} %param.31) | copy-start | bytes 9437188
  7.2 6.1 %copy-start.1 = (bf16[16,2048]{1,0:T(8,128)(2,1)S(1)}, bf16[16,2048]{1,0:T(8,128)(2,1)}, u32[]{:S(2)}) copy-start(bf16[16,2048]{1,0:T(8,128)(2,1)} %param.16) | copy-start | bytes 196612
  7.2 6.1 %copy-start.4 = (f32[2048]{0:T(1024)S(1)}, f32[2048]{0:T(1024)}, u32[]{:S(2)}) copy-start(f32[2048]{0:T(1024)} %param.17) | copy-start | bytes 24580
  7.2 40.9 %all-reduce.2.cloned.1.call-start = ((), (), s32[]{:S(2)}) async-start(), calls=%async_computation.3 | async-start | bytes 131072 | tf_op jit(solution)/shard_map/psum | solution.py:61
  8.4 7.0 %copy-start.7 = (f32[512]{0:T(512)S(1)}, f32[512]{0:T(512)}, u32[]{:S(2)}) copy-start(f32[512]{0:T(512)} %param.22) | copy-start | bytes 6148
  15.4 8.3 %copy-start.9 = (f32[128]{0:T(128)S(1)}, f32[128]{0:T(128)}, u32[]{:S(2)}) copy-start(f32[128]{0:T(128)} %param.23) | copy-start | bytes 1540
  23.5 4.0 %copy-start.5 = (s32[16,2]{0,1:T(2,128)S(1)}, s32[16,2]{0,1:T(2,128)}, u32[]{:S(2)}) copy-start(s32[16,2]{0,1:T(2,128)} %param.27) | copy-start | bytes 388
  23.6 25.6 %copy-start.6 = (f32[2048]{0:T(1024)S(1)}, f32[2048]{0:T(1024)}, u32[]{:S(2)}) copy-start(f32[2048]{0:T(1024)} %param.26) | copy-start | bytes 24580
  27.5 71.8 %reduce-scatter.2.cloned.1.call-start = ((), (), s32[]{:S(2)}) async-start(), calls=%async_computation.4 | async-start | bytes 1572864 | tf_op jit(solution)/shard_map/reduce_scatter | solution.py:93
  48.1 36.9 %copy-start.10 = (bf16[1,2048,768]{2,1,0:T(8,128)(2,1)S(1)}, bf16[1,2048,768]{2,1,0:T(8,128)(2,1)}, u32[]{:S(2)}) copy-start(bf16[1,2048,768]{2,1,0:T(8,128)(2,1)} %param.29) | copy-start | bytes 9437188
  83.9 1.0 copy-start.2
  86.8 34.9 %copy-start.8 = (f32[16,2]{0,1:T(2,128)S(1)}, f32[16,2]{0,1:T(2,128)}, u32[]{:S(2)}) copy-start(f32[16,2]{0,1:T(2,128)} %param.28) | copy-start | bytes 388
  86.8 42.4 %copy-start.3 = (bf16[16,2048]{1,0:T(8,128)(2,1)S(1)}, bf16[16,2048]{1,0:T(8,128)(2,1)}, u32[]{:S(2)}) copy-start(bf16[16,2048]{1,0:T(8,128)(2,1)} %all-reduce.2.cloned.1.call-done) | copy-start | bytes 196612
  92.4 36.9 %all-gather.2.cloned.1.call-start = ((), (), s32[]{:S(2)}) async-start(), calls=%async_computation.5 | async-start | bytes 1572864 | tf_op jit(solution)/shard_map/all_gather | solution.py:98
Sparse Core Ops, SparseCore 0:
  27.6 20.4 all-reduce.1
  92.5 6.7 reduce-scatter.1
  121.8 7.4 all-gather.1
where the time goes:
time: 139 us; the launch traced here: 138 us
  blocking collectives  55.7 us (40%)
  waiting for transfers between devices  34.1 us (25%)
  matrix products  21 us (15%)
  between operations  14 us (10%)
  other arithmetic  11.7 us (8%)
  local copies, waits for them, and re-layouts  1.53 us (1%)
    all_to_all x1, blocking collectives, on_device(): lax.all_to_all(outgoing, 'ep', split_axis=0, concat_axis=0, tiled=True)  33.3 us
    all_to_all x1, blocking collectives, on_device(): lax.all_to_all(answer, 'ep', split_axis=0, concat_axis=0, tiled=True)  22.4 us
    psum x1, waiting for transfers between devices, on_device(): lax.psum(jnp.dot(gated, w_output, preferred_element_type=jnp.float32).ast...  19.8 us
    reduce_sum x1, other arithmetic, on_device(): readout = jnp.sum(query_part[..., None] * new_state, axis=2)  8.11 us
    all_gather x1, waiting for transfers between devices, on_device(): returned = lax.all_gather(returned, 'tp', axis=2, tiled=True)  7.45 us
    reduce_scatter x1, waiting for transfers between devices, on_device(): lax.psum_scatter(partial_down.astype(jnp.bfloat16), 'tp', scatter_dimensi...  6.85 us
    dot_general x1, matrix products, on_device(): jnp.dot(activated, w_exp_down[0], preferred_element_type=jnp.float32)  5.54 us
    dot_general x1, matrix products, on_device(): jnp.dot(gated, w_output, preferred_element_type=jnp.float32)  3.65 us
  transfers between devices with their start and end apart: 3, of which 3 were waited for; matrix products, arithmetic and copies ran while one was open for 1% of the time, Pallas kernels for 0%

commit v1 on v0

--- a/solution.py
+++ b/solution.py
@@ -58,8 +58,11 @@
         .reshape(seq_dev, head_width)
         .astype(jnp.bfloat16)
     )
-    mixed_out = lax.psum(
-        jnp.dot(gated, w_output, preferred_element_type=jnp.float32).astype(jnp.bfloat16), "tp"
+    mixed_out = jnp.sum(
+        lax.all_gather(
+            jnp.dot(gated, w_output, preferred_element_type=jnp.float32).astype(jnp.bfloat16), "tp"
+        ),
+        axis=0,
     ).astype(jnp.float32)
     middle = (residual + mixed_out).astype(jnp.bfloat16)
     normed_two = rms_scale(middle.astype(jnp.float32), moe_gain).astype(jnp.bfloat16)

time: 139 us -> 120 us (0.86)
  waiting for transfers between devices: 34.1 us -> 14.3 us
  blocking collectives: 55.7 us -> 59.2 us
  matrix products: 21 us -> 19.5 us
    psum x1 -> x0, waiting for transfers between devices: 19.8 us -> none  [on_device(): lax.psum(jnp.dot(gated, w_output, preferred_element_type=jnp.float32).ast...]
    all_gather x0 -> x1, blocking collectives: none -> 2.03 us  [on_device(): lax.all_gather(jnp.dot(gated, w_output, preferred_element_type=jnp.float3...]
    all_to_all x1, blocking collectives: 33.3 us -> 34.8 us  [on_device(): lax.all_to_all(outgoing, 'ep', split_axis=0, concat_axis=0, tiled=True)]
  transfers between devices with their start and end apart: 3 -> 2, of which waited for: 3 -> 2; matrix products, arithmetic and copies ran while one was open for 1% -> 0% of each run, Pallas kernels for 0% -> 0%
where the time goes in v1:
time: 120 us
  blocking collectives  59.2 us (49%)
  matrix products  19.5 us (16%)
  waiting for transfers between devices  14.3 us (12%)
  between operations  14.3 us (12%)
  other arithmetic  10.8 us (9%)
  local copies, waits for them, and re-layouts  1.53 us (1%)
    all_to_all x1, blocking collectives, on_device(): lax.all_to_all(outgoing, 'ep', split_axis=0, concat_axis=0, tiled=True)  34.8 us
    all_to_all x1, blocking collectives, on_device(): lax.all_to_all(answer, 'ep', split_axis=0, concat_axis=0, tiled=True)  22.4 us
    reduce_sum x1, other arithmetic, on_device(): readout = jnp.sum(query_part[..., None] * new_state, axis=2)  8.11 us
    all_gather x1, waiting for transfers between devices, on_device(): returned = lax.all_gather(returned, 'tp', axis=2, tiled=True)  7.45 us
    reduce_scatter x1, waiting for transfers between devices, on_device(): lax.psum_scatter(partial_down.astype(jnp.bfloat16), 'tp', scatter_dimensi...  6.82 us
    dot_general x1, matrix products, on_device(): jnp.dot(activated, w_exp_down[0], preferred_element_type=jnp.float32)  5.52 us
    dot_general x1, matrix products, on_device(): jnp.dot(gated, w_output, preferred_element_type=jnp.float32)  3.01 us
  transfers between devices with their start and end apart: 2, of which 2 were waited for; matrix products, arithmetic and copies ran while one was open for 0% of the time, Pallas kernels for 0%

profile of v1, /device:TPU:0, one launch (start us, length us, event | category | flops | bytes accessed | tf_op | source)
XLA Modules:
  0.0 119.6 jit_solution(7668793679527051703)
XLA Ops:
  7.2 0.0 copy-start
  7.2 0.0 copy-start.1
  7.2 0.0 copy-start.3
  7.2 0.0 reduce-scatter.2.cloned.1.call-start
  7.3 1.1 fusion.19
  8.4 0.0 copy-start.6
  8.4 2.1 %add_divide_fusion.1 = (f32[16,512]{1,0:T(8,128)S(1)}, f32[16,512]{1,0:T(8,128)S(1)}) fusion(bf16[2048,512]{1,0:T(8,128)(2,1)} %param.19, bf16[16,2048]{1,0:T(8,128)(2,1)} %param.16, f32[2048]{0:T(1024)} %param.17, f32[16]{0:T(128)S(1)} %add_rsqrt_fusion.2), kind=kOutput, calls=%fused_computation.37 | convolution fusion | flops 33726464 | bytes 2236480 | tf_op jit(solution)/shard_map/dot_general | solution.py:42
  10.6 0.7 broadcast_subtract_fusion
  11.2 2.1 %fusion.47 = f32[16,512]{1,0:T(8,128)S(1)} fusion(bf16[2048,512]{1,0:T(8,128)(2,1)} %param.18, bf16[16,2048]{1,0:T(8,128)(2,1)} %param.16, f32[2048]{0:T(1024)} %param.17, f32[16]{0:T(128)S(1)} %add_rsqrt_fusion.2), kind=kOutput, calls=%fused_computation.69 | convolution fusion | flops 33685504 | bytes 2203712 | tf_op jit(solution)/shard_map/dot_general | solution.py:39
  13.3 0.0 copy-done.1
  13.3 0.0 copy-done.3
  13.3 2.0 %fusion.43 = f32[16,512]{1,0:T(8,128)S(1)} fusion(bf16[2048,512]{1,0:T(8,128)(2,1)} %param.20, bf16[16,2048]{1,0:T(8,128)(2,1)S(1)} %copy-done.1, f32[2048]{0:T(1024)S(1)} %copy-done.3, f32[16]{0:T(128)S(1)} %add_rsqrt_fusion.2), kind=kOutput, calls=%fused_computation.67 | convolution fusion | flops 33685504 | bytes 2203712 | tf_op jit(solution)/shard_map/dot_general | solution.py:45
  15.4 0.0 copy-done.6
  15.4 0.0 copy-start.8
  15.4 8.1 %multiply_reduce_fusion = (f32[16,4,128]{2,1,0:T(4,128)S(1)}, f32[16,4,128,128]{3,2,1,0:T(8,128)}) fusion(f32[16,4,128]{2,1,0:T(4,128)S(1)} %mul.153, f32[16,4,128]{2,1,0:T(4,128)S(1)} %mul.161, f32[16,4,128]{2,1,0:T(4,128)S(1)} %bitcast.57, f32[16,4,128,128]{3,2,1,0:T(8,128)} %param.24, f32[16,4,128]{2,1,0:T(4,128)S(1)} %bitcast.56), kind=kLoop, calls=%fused_computation | loop fusion | flops 5234688 | bytes 8552448 | tf_op jit(solution)/shard_map/reduce_sum | solution.py:55
  23.6 0.0 copy-start.4
  23.6 0.0 copy-start.5
  23.6 0.1 multiply_reduce_fusion.1
  23.7 0.1 broadcast_multiply_fusion
  23.8 0.0 copy-done.8
  23.8 3.0 %convolution_convert_fusion.1 = bf16[16,2048]{1,0:T(8,128)(2,1)S(1)} fusion(bf16[512,2048]{1,0:T(8,128)(2,1)} %param.25, f32[2,8,4,128]{3,2,1,0:T(4,128)S(1)} %bitcast.58, f32[512]{0:T(512)S(1)} %broadcast_bitcast_fusion, bf16[2048,512]{1,0:T(8,128)(2,1)} %param.21, bf16[16,2048]{1,0:T(8,128)(2,1)S(1)} %copy-done.1, f32[2048]{0:T(1024)S(1)} %copy-done.3, ...), kind=kOutput, calls=%fused_computation.12 | convolution fusion | flops 67330048 | bytes 4368448 | tf_op jit(solution)/shard_map/dot_general | solution.py:63
  26.8 2.0 %all-gather = bf16[32,2048]{1,0:T(8,128)(2,1)S(1)} all-gather(bf16[16,2048]{1,0:T(8,128)(2,1)S(1)} %convolution_convert_fusion.1), channel_id=2, replica_groups=mesh['ep'=16,'tp'=2] {'tp'}, dimensions={0}, use_global_device_ids=true | all-gather | bytes 196608 | tf_op jit(solution)/shard_map/all_gather | solution.py:62
  28.9 0.1 fusion.23
  29.0 0.0 copy-done.4
  29.0 0.1 copy.24
  29.1 0.1 eq.53
  29.2 0.1 fusion.33
  29.3 0.1 reduce_window_sum.11
  29.3 0.2 select_reduce_fusion.1
  29.5 0.1 eq.57
  29.6 0.1 copy.25
  29.7 0.0 copy-start.9
  29.7 0.1 fusion.31
  29.8 0.0 copy-done.5
  29.8 0.5 convolution_convert_fusion
  30.3 34.8 %all_to_all.10 = bf16[16,16,2048]{2,1,0:T(8,128)(2,1)S(1)} all-to-all(bf16[16,16,2048]{2,1,0:T(8,128)(2,1)S(1)} %bitcast.50), channel_id=1, replica_groups=mesh['ep'=16,'tp'=2] {'ep'}, dimensions={0} | all-to-all | bytes 2097152 | tf_op jit(solution)/shard_map/all_to_all | solution.py:89
  65.1 0.0 copy-start.2
  65.1 1.0 copy-done.2
  66.1 0.0 copy-done.9
  66.1 1.9 %fusion.4 = f32[256,768]{1,0:T(8,128)} fusion(bf16[256,2048]{1,0:T(8,128)(2,1)S(1)} %bitcast.52, bf16[1,2048,768]{2,1,0:T(8,128)(2,1)S(1)} %copy-done.9), kind=kOutput, calls=%fused_computation.6 | convolution fusion | flops 805306368 | bytes 4980736 | tf_op jit(solution)/shard_map/dot_general | solution.py:92
  68.0 0.0 copy-done
  68.0 0.0 copy-start.7
  68.0 5.5 %fusion.6 = bf16[256,2048]{1,0:T(8,128)(2,1)} fusion(bf16[1,768,2048]{2,1,0:T(8,128)(2,1)S(1)} %copy-done, bf16[256,2048]{1,0:T(8,128)(2,1)} %bitcast.53, bf16[1,2048,768]{2,1,0:T(8,128)(2,1)} %param.30, f32[256,768]{1,0:T(8,128)} %fusion.4), kind=kOutput, calls=%fused_computation.9 | convolution fusion | flops 1612316672 | bytes 9175040 | tf_op jit(solution)/shard_map/dot_general | solution.py:95
  73.5 0.0 reduce-scatter.2.cloned.1.call-update
  73.5 0.0 all-gather.3.cloned.1.call-start
  73.6 6.8 %reduce-scatter.2.cloned.1.call-done = bf16[256,1024]{1,0:T(8,128)(2,1)} async-done(((bf16[256,2048]{1,0:T(8,128)(2,1)}), bf16[256,1024]{1,0:T(8,128)(2,1)}) %reduce-scatter.2.cloned.1.call-update) | async-done | bytes 524304 | tf_op jit(solution)/shard_map/reduce_scatter | solution.py:96
  80.4 22.4 %all_to_all.11 = bf16[16,16,1024]{2,1,0:T(8,128)(2,1)} all-to-all(bf16[16,16,1024]{2,1,0:T(8,128)(2,1)} %bitcast.55), channel_id=1, replica_groups=mesh['ep'=16,'tp'=2] {'ep'}, dimensions={0} | all-to-all | bytes 1048576 | tf_op jit(solution)/shard_map/all_to_all | solution.py:100
  102.8 0.0 all-gather.3.cloned.1.call-update
  102.8 0.0 copy-done.7
  102.8 0.1 select_reduce_fusion
  102.9 7.4 %all-gather.3.cloned.1.call-done = bf16[16,16,2048]{2,1,0:T(8,128)(2,1)} async-done(((bf16[16,16,1024]{2,1,0:T(8,128)(2,1)}), bf16[16,16,2048]{2,1,0:T(8,128)(2,1)}) %all-gather.3.cloned.1.call-update) | async-done | bytes 1048592 | tf_op jit(solution)/shard_map/all_gather | solution.py:101
  110.4 2.4 %fusion.9 = bf16[16,2048]{1,0:T(8,128)(2,1)} fusion(f32[256,16]{0,1:T(8,128)S(1)} %select_reduce_fusion, bf16[256,2048]{1,0:T(8,128)(2,1)} %bitcast.51, bf16[16,2048]{1,0:T(8,128)(2,1)S(1)} %reduce_sum.69, bf16[16,2048]{1,0:T(8,128)(2,1)S(1)} %copy-done.1), kind=kOutput, calls=%fused_computation.11 | convolution fusion | flops 100892672 | bytes 1261568 | tf_op jit(solution)/shard_map/dot_general | solution.py:106
  (15 shorter events, 0.2 us)
Async XLA Ops:
  7.2 60.8 %copy-start = (bf16[1,768,2048]{2,1,0:T(8,128)(2,1)S(1)}, bf16[1,768,2048]{2,1,0:T(8,128)(2,1)}, u32[]{:S(2)}) copy-start(bf16[1,768,2048]{2,1,0:T(8,128)(2,1)} %param.31) | copy-start | bytes 9437188
  7.2 6.2 %copy-start.1 = (bf16[16,2048]{1,0:T(8,128)(2,1)S(1)}, bf16[16,2048]{1,0:T(8,128)(2,1)}, u32[]{:S(2)}) copy-start(bf16[16,2048]{1,0:T(8,128)(2,1)} %param.16) | copy-start | bytes 196612
  7.2 6.2 %copy-start.3 = (f32[2048]{0:T(1024)S(1)}, f32[2048]{0:T(1024)}, u32[]{:S(2)}) copy-start(f32[2048]{0:T(1024)} %param.17) | copy-start | bytes 24580
  7.2 73.2 %reduce-scatter.2.cloned.1.call-start = ((), (), s32[]{:S(2)}) async-start(), calls=%async_computation.3 | async-start | bytes 1572864 | tf_op jit(solution)/shard_map/reduce_scatter | solution.py:96
  8.4 7.0 %copy-start.6 = (f32[512]{0:T(512)S(1)}, f32[512]{0:T(512)}, u32[]{:S(2)}) copy-start(f32[512]{0:T(512)} %param.22) | copy-start | bytes 6148
  15.4 8.3 %copy-start.8 = (f32[128]{0:T(128)S(1)}, f32[128]{0:T(128)}, u32[]{:S(2)}) copy-start(f32[128]{0:T(128)} %param.23) | copy-start | bytes 1540
  23.6 5.5 %copy-start.4 = (s32[16,2]{0,1:T(2,128)S(1)}, s32[16,2]{0,1:T(2,128)}, u32[]{:S(2)}) copy-start(s32[16,2]{0,1:T(2,128)} %param.27) | copy-start | bytes 388
  23.6 6.2 %copy-start.5 = (f32[2048]{0:T(1024)S(1)}, f32[2048]{0:T(1024)}, u32[]{:S(2)}) copy-start(f32[2048]{0:T(1024)} %param.26) | copy-start | bytes 24580
  29.7 36.4 %copy-start.9 = (bf16[1,2048,768]{2,1,0:T(8,128)(2,1)S(1)}, bf16[1,2048,768]{2,1,0:T(8,128)(2,1)}, u32[]{:S(2)}) copy-start(bf16[1,2048,768]{2,1,0:T(8,128)(2,1)} %param.29) | copy-start | bytes 9437188
  65.1 1.0 copy-start.2
  68.0 34.8 %copy-start.7 = (f32[16,2]{0,1:T(2,128)S(1)}, f32[16,2]{0,1:T(2,128)}, u32[]{:S(2)}) copy-start(f32[16,2]{0,1:T(2,128)} %param.28) | copy-start | bytes 388
  73.5 36.8 %all-gather.3.cloned.1.call-start = ((), (), s32[]{:S(2)}) async-start(), calls=%async_computation.4 | async-start | bytes 1572864 | tf_op jit(solution)/shard_map/all_gather | solution.py:101
Sparse Core Ops, SparseCore 0:
  73.7 6.7 reduce-scatter.1
  102.9 7.4 all-gather.2
